TPU v7x, 32 devices: a whole 2x2x4 slice. The times are simulated.
32 devices in a mesh: sp: 8 (over z, y), tp: 4 (over x, core).
Axes of the slice: x: 2, y: 2, z: 4, core: 2. Of those that a mesh axis runs over, the one named last changes fastest.
Arguments:
- queries: bfloat16 [4096, 1024], P('sp', 'tp'), may hold values from -200 to 200
- keys: bfloat16 [4096, 1024], P('sp', 'tp'), may hold values from -6 to 6
- values: bfloat16 [4096, 1024], P('sp', 'tp'), may hold values from -24 to 24
- cum_gate: float32 [4096, 8], P('sp', 'tp'), may hold values from -414 to 0, as said below
- residual: bfloat16 [4096, 2048], P(('sp', 'tp')), may hold values from -1.5 to 1.5
- w_out: bfloat16 [1024, 2048], replicated, may hold values from -0.1875 to 0.1875
- gain: float32 [2048], replicated, may hold values from 0.1 to 1.9
- w_up: bfloat16 [2048, 8192], P('sp', 'tp'), may hold values from -0.125 to 0.125
- w_down: bfloat16 [8192, 2048], P('tp', 'sp'), may hold values from -0.0625 to 0.0625
Outputs:
- output: bfloat16 [4096, 2048], P(('sp', 'tp'))
Inputs may be any that keep to these rules, and one draw needn't show every extreme that they name: Within each head, cum_gate never rises from one position to the next.
All inputs are finite; a program needn't handle non-finite values.
Results may differ from a plain program's by a relative error of at most 0.022.
Values may be sent and summed in bfloat16 or wider, within the bound.
A program may use at most 128 MiB of HBM per device.

v0:
```python
import math
import jax
import jax.numpy as jnp
from jax import lax
from jax.sharding import PartitionSpec as P


def per_device(queries, keys, values, cum_gate, residual, w_out, gain, w_up, w_down):
    tok_rows, width = queries.shape
    heads_here = cum_gate.shape[1]
    head_size = width // heads_here
    score_scale = head_size ** (-0.5)
    row_offset = lax.axis_index("sp") * tok_rows
    query_heads = queries.reshape(tok_rows, heads_here, head_size)
    query_pos = row_offset + jnp.arange(tok_rows, dtype=jnp.int32)
    all_gates = lax.all_gather(cum_gate, "sp", axis=0, tiled=True)
    initial = (
        jnp.full((tok_rows, heads_here), -1e30, jnp.float32),
        jnp.zeros((tok_rows, heads_here), jnp.float32),
        jnp.zeros((tok_rows, heads_here, head_size), jnp.float32),
    )
    carried = initial
    key_rows = lax.all_gather(keys, "sp", axis=0, tiled=True)
    value_rows = lax.all_gather(values, "sp", axis=0, tiled=True)
    row_count = key_rows.shape[0]
    span_rows = math.gcd(row_count, 2048)
    block_count = row_count // span_rows
    key_blocks = key_rows.reshape(block_count, span_rows, heads_here, head_size)
    value_blocks = value_rows.reshape(block_count, span_rows, heads_here, head_size)
    first_pos = jnp.arange(block_count, dtype=jnp.int32) * span_rows

    def absorb_block(running, packed):
        running_max, running_sum, accumulated = running
        key_blk, value_blk, block_start = packed
        gate_blk = lax.dynamic_slice_in_dim(all_gates, block_start, span_rows, 0)
        scores = jnp.einsum(
            "qhd,khd->qhk", query_heads, key_blk, preferred_element_type=jnp.float32
        )
        scores = scores * score_scale + cum_gate[:, :, None] - gate_blk.T[None, :, :]
        key_pos = block_start + jnp.arange(span_rows, dtype=jnp.int32)
        scores = jnp.where(key_pos[None, None, :] <= query_pos[:, None, None], scores, -1e30)
        new_max = jnp.maximum(running_max, jnp.max(scores, axis=-1))
        rescale = jnp.exp(running_max - new_max)
        weights = jnp.exp(scores - new_max[:, :, None])
        running_sum = running_sum * rescale + jnp.sum(weights, axis=-1)
        product = jnp.einsum(
            "qhk,khd->qhd",
            weights.astype(jnp.bfloat16),
            value_blk,
            preferred_element_type=jnp.float32,
        )
        accumulated = accumulated * rescale[:, :, None] + product
        return ((new_max, running_sum, accumulated), None)

    carried, _ = lax.scan(absorb_block, carried, (key_blocks, value_blocks, first_pos))
    running_max, running_sum, accumulated = carried
    attended = (accumulated / running_sum[:, :, None]).reshape(tok_rows, width).astype(jnp.bfloat16)
    mine = lax.all_to_all(attended, "tp", split_axis=0, concat_axis=1, tiled=True)
    projected = jnp.dot(mine, w_out, preferred_element_type=jnp.float32)
    residual_sum = residual.astype(jnp.float32) + projected
    mean_square = jnp.mean(residual_sum * residual_sum, axis=-1, keepdims=True)
    normed = (residual_sum * lax.rsqrt(mean_square + 1e-06) * gain).astype(jnp.bfloat16)
    normed_all = lax.all_gather(normed, "tp", axis=0, tiled=True)
    up_proj = jnp.dot(
        normed_all,
        lax.all_gather(w_up, "sp", axis=0, tiled=True),
        preferred_element_type=jnp.float32,
    )
    hidden = jnp.square(jax.nn.relu(up_proj)).astype(jnp.bfloat16)
    down_whole = lax.all_gather(w_down, "sp", axis=1, tiled=True)
    rounded = jnp.dot(hidden, down_whole, preferred_element_type=jnp.float32).astype(jnp.bfloat16)
    branch_out = lax.psum_scatter(
        lax.optimization_barrier(rounded).astype(jnp.float32).astype(jnp.bfloat16),
        "tp",
        scatter_dimension=0,
        tiled=True,
    ).astype(jnp.float32)
    return (residual_sum + branch_out).astype(jnp.bfloat16)


def solution(mesh):
    return jax.shard_map(
        per_device,
        mesh=mesh,
        in_specs=(
            P("sp", "tp"),
            P("sp", "tp"),
            P("sp", "tp"),
            P("sp", "tp"),
            P(("sp", "tp"), None),
            P(),
            P(),
            P("sp", "tp"),
            P("tp", "sp"),
        ),
        out_specs=P(("sp", "tp"), None),
        check_vma=False,
    )
```

profile of v0, /device:TPU:0, one launch (start us, length us, event | category | flops | bytes accessed | tf_op | source)
XLA Modules:
  0.0 501.9 jit_solution(15590965651173478988)
XLA Ops:
  6.5 0.0 copy-start
  6.5 0.0 all-gather.6.cloned.1.call-start
  6.5 0.7 all-gather.6.cloned.1.call-update
  7.3 0.0 all-gather.8.cloned.1.call-start
  7.3 0.7 all-gather.8.cloned.1.call-update
  8.0 0.0 all-gather.10.cloned.1.call-start
  8.1 1.1 copy.17
  9.2 0.2 copy.19
  9.4 32.7 %all_gather.19 = f32[4096,2]{0,1:T(2,128)S(1)} all-gather(f32[512,2]{0,1:T(2,128)} %param.14), channel_id=1, replica_groups=mesh['sp'=8,'tp'=4] {'sp'}, dimensions={0}, use_global_device_ids=true | all-gather | bytes 36864 | tf_op jit(solution)/shard_map/all_gather | solution.py:16
  42.0 19.4 %all-gather.6.cloned.1.call-done = bf16[4096,256]{1,0:T(8,128)(2,1)} async-done(((bf16[512,256]{1,0:T(8,128)(2,1)}), bf16[4096,256]{1,0:T(8,128)(2,1)}) %all-gather.6.cloned.1.call-update) | async-done | bytes 2097168 | tf_op jit(solution)/shard_map/all_gather | solution.py:23
  61.4 4.0 reshape.62
  65.4 45.8 %all-gather.8.cloned.1.call-done = bf16[4096,256]{1,0:T(8,128)(2,1)} async-done(((bf16[512,256]{1,0:T(8,128)(2,1)}), bf16[4096,256]{1,0:T(8,128)(2,1)}) %all-gather.8.cloned.1.call-update) | async-done | bytes 2097168 | tf_op jit(solution)/shard_map/all_gather | solution.py:24
  111.2 4.0 reshape.64
  115.2 0.0 copy-done
  115.2 45.9 %while.15 = (s32[]{:T(128)}, f32[512,2]{0,1:T(2,128)S(1)}, f32[512,2]{0,1:T(2,128)S(1)}, f32[512,2,128]{0,2,1:T(8,128)}, s32[2]{0:T(128)S(1)}, /*index=5*/bf16[2...) while((s32[]{:T(128)}, f32[512,2]{0,1:T(2,128)S(1)}, ...), condition=%wide.region_3.4_spmd.clone, body=%wide.region_0.3_spmd.clone.sunk | while | flops 1110842880 | bytes 39239884 | solution.py:55
  115.2 0.6 dynamic_slice.26
  117.4 0.1 dynamic-slice_bitcast_fusion.2
  117.5 0.6 iota_add_fusion.5
  118.1 0.8 broadcast_compare_fusion.2
  118.9 2.7 constant_dynamic-slice_fusion.3
  121.6 4.6 fusion.40
  126.2 4.8 fusion.42
  131.0 0.8 copy.34
  131.8 6.2 %fusion.44 = f32[512,2,128]{0,2,1:T(8,128)} fusion(f32[2,2048,512]{2,1,0:T(8,128)} %get-tuple-element.231, f32[512,2]{0,1:T(2,128)S(1)} %fusion.41, f32[2,2048]{1,0:T(2,128)S(1)} %dynamic-slice_bitcast_fusion.2, f32[512,2]{0,1:T(2,128)S(1)} %get-tuple-element.270, pred[512,2048]{0,1:T(8,128)(4,1)S(1)} %broadcast_compare_fusion.2, ...), kind=kOutput, calls=%fused_computation.12.clone.1 | convolution fusion | flops 549847040 | bytes 11563009 | tf_op jit(solution)/shard_map/while/body/eval_jaxpr/qhk,khd->qhd/dot_general | solution.py:46
  138.1 0.6 dynamic_slice.26
  140.3 0.1 dynamic-slice_bitcast_fusion.2
  140.4 0.6 iota_add_fusion.5
  141.0 0.8 broadcast_compare_fusion.2
  141.8 2.7 constant_dynamic-slice_fusion.3
  144.5 4.6 fusion.40
  149.1 4.8 fusion.42
  153.9 0.8 copy.34
  154.7 6.4 %fusion.44 = f32[512,2,128]{0,2,1:T(8,128)} fusion(f32[2,2048,512]{2,1,0:T(8,128)} %get-tuple-element.231, f32[512,2]{0,1:T(2,128)S(1)} %fusion.41, f32[2,2048]{1,0:T(2,128)S(1)} %dynamic-slice_bitcast_fusion.2, f32[512,2]{0,1:T(2,128)S(1)} %get-tuple-element.270, pred[512,2048]{0,1:T(8,128)(4,1)S(1)} %broadcast_compare_fusion.2, ...), kind=kOutput, calls=%fused_computation.12.clone.1 | convolution fusion | flops 549847040 | bytes 11563009 | tf_op jit(solution)/shard_map/while/body/eval_jaxpr/qhk,khd->qhd/dot_general | solution.py:46
  161.1 0.0 copy-start.1
  161.1 1.1 divide_convert_fusion
  162.2 0.1 reshape.65
  162.2 0.2 copy.24
  162.4 8.5 %all_to_all.16 = bf16[4,128,256]{2,1,0:T(8,128)(2,1)S(1)} all-to-all(bf16[4,128,256]{2,1,0:T(8,128)(2,1)S(1)} %copy.24), channel_id=1, replica_groups=mesh['sp'=8,'tp'=4] {'tp'}, dimensions={0} | all-to-all | bytes 524288 | tf_op jit(solution)/shard_map/all_to_all | solution.py:58
  171.0 0.2 copy.22
  171.1 3.1 multiply_reduce_fusion
  174.3 0.0 copy-done.1
  174.3 0.9 multiply_convert_fusion.1
  175.2 0.0 all-gather.10.cloned.1.call-update
  175.3 0.0 all-gather.12.cloned.1.call-start
  175.3 0.5 all-gather.12.cloned.1.call-update
  175.8 0.0 all-gather.14.cloned.1.call-start
  175.9 0.5 all-gather.14.cloned.1.call-update
  176.4 0.2 reduce-scatter.2.cloned.1.call-start
  176.7 19.0 %all-gather.10.cloned.1.call-done = bf16[512,2048]{1,0:T(8,128)(2,1)} async-done(((bf16[128,2048]{1,0:T(8,128)(2,1)}), bf16[512,2048]{1,0:T(8,128)(2,1)}) %all-gather.10.cloned.1.call-update) | async-done | bytes 2097168 | tf_op jit(solution)/shard_map/all_gather | solution.py:63
  195.6 126.5 %all-gather.12.cloned.1.call-done = bf16[2048,2048]{1,0:T(8,128)(2,1)} async-done(((bf16[256,2048]{1,0:T(8,128)(2,1)}), bf16[2048,2048]{1,0:T(8,128)(2,1)}) %all-gather.12.cloned.1.call-update) | async-done | bytes 8388624 | tf_op jit(solution)/shard_map/all_gather | solution.py:66
  322.1 125.0 %all-gather.14.cloned.1.call-done = bf16[2048,2048]{1,0:T(8,128)(2,1)} async-done(((bf16[2048,256]{1,0:T(8,128)(2,1)}), bf16[2048,2048]{1,0:T(8,128)(2,1)}) %all-gather.14.cloned.1.call-update) | async-done | bytes 8388624 | tf_op jit(solution)/shard_map/all_gather | solution.py:70
  447.1 16.5 %convolution_convert_fusion = bf16[512,2048]{1,0:T(8,128)(2,1)} fusion(bf16[2048,2048]{1,0:T(8,128)(2,1)} %all-gather.14.cloned.1.call-done, bf16[512,2048]{1,0:T(8,128)(2,1)} %all-gather.10.cloned.1.call-done, bf16[2048,2048]{1,0:T(8,128)(2,1)} %all-gather.12.cloned.1.call-done), kind=kOutput, calls=%fused_computation.30 | convolution fusion | flops 8594128896 | bytes 20971520 | tf_op jit(solution)/shard_map/dot_general | solution.py:71
  463.7 0.0 reduce-scatter.2.cloned.1.call-update
  463.7 29.5 %reduce-scatter.2.cloned.1.call-done = bf16[128,2048]{1,0:T(8,128)(2,1)} async-done(((bf16[512,2048]{1,0:T(8,128)(2,1)}), bf16[128,2048]{1,0:T(8,128)(2,1)}) %reduce-scatter.2.cloned.1.call-update) | async-done | bytes 524304 | tf_op jit(solution)/shard_map/reduce_scatter | solution.py:72
  493.2 1.9 add_convert_fusion
  (13 shorter events, 0.1 us)
Async XLA Ops:
  6.5 108.6 %copy-start = (f32[512,2]{0,1:T(2,128)S(1)}, f32[512,2]{0,1:T(2,128)}, u32[]{:S(2)}) copy-start(f32[512,2]{0,1:T(2,128)} %param.14) | copy-start | bytes 12292
  6.5 54.9 %all-gather.6.cloned.1.call-start = ((), (), s32[]{:S(2)}) async-start(), calls=%async_computation.2 | async-start | bytes 2359296 | tf_op jit(solution)/shard_map/all_gather | solution.py:23
  7.3 103.9 %all-gather.8.cloned.1.call-start = ((), (), s32[]{:S(2)}) async-start(), calls=%async_computation.3 | async-start | bytes 2359296 | tf_op jit(solution)/shard_map/all_gather | solution.py:24
  8.0 187.6 %all-gather.10.cloned.1.call-start = ((), (), s32[]{:S(2)}) async-start(), calls=%async_computation.4 | async-start | bytes 2621440 | tf_op jit(solution)/shard_map/all_gather | solution.py:63
  161.1 13.2 %copy-start.1 = (f32[2048]{0:T(1024)S(1)}, f32[2048]{0:T(1024)}, u32[]{:S(2)}) copy-start(f32[2048]{0:T(1024)} %param.17) | copy-start | bytes 24580
  175.3 146.8 %all-gather.12.cloned.1.call-start = ((), (), s32[]{:S(2)}) async-start(), calls=%async_computation.5 | async-start | bytes 9437184 | tf_op jit(solution)/shard_map/all_gather | solution.py:66
  175.8 271.3 %all-gather.14.cloned.1.call-start = ((), (), s32[]{:S(2)}) async-start(), calls=%async_computation.6 | async-start | bytes 9437184 | tf_op jit(solution)/shard_map/all_gather | solution.py:70
  176.4 316.7 %reduce-scatter.2.cloned.1.call-start = ((), (), s32[]{:S(2)}) async-start(), calls=%async_computation.7 | async-start | bytes 2621440 | tf_op jit(solution)/shard_map/reduce_scatter | solution.py:72
Sparse Core Ops, SparseCore 0:
  9.5 51.9 all-gather.5
  63.5 47.6 all-gather.7
  175.4 20.1 all-gather.9
  197.6 124.4 all-gather.11
  324.0 123.1 all-gather.13
  463.8 29.3 reduce-scatter.1
where the time goes:
time: 502 us
  waiting for transfers between devices  368 us (73%)
  matrix products  41.4 us (8%)
  blocking collectives  41.2 us (8%)
  local copies, waits for them, and re-layouts  18 us (4%)
  other arithmetic  16.3 us (3%)
  between operations  13.6 us (3%)
    all_gather x1, waiting for transfers between devices, per_device(): lax.all_gather(w_up, 'sp', axis=0, tiled=True)  126 us
    all_gather x1, waiting for transfers between devices, per_device(): down_whole = lax.all_gather(w_down, 'sp', axis=1, tiled=True)  125 us
    all_gather x1, waiting for transfers between devices, per_device(): value_rows = lax.all_gather(values, 'sp', axis=0, tiled=True)  45.8 us
    all_gather x1, blocking collectives, per_device(): all_gates = lax.all_gather(cum_gate, 'sp', axis=0, tiled=True)  32.7 us
    reduce_scatter x1, waiting for transfers between devices, per_device(): lax.psum_scatter(lax.optimization_barrier(rounded).astype(jnp.float32).as...  29.5 us
    all_gather x1, waiting for transfers between devices, per_device(): key_rows = lax.all_gather(keys, 'sp', axis=0, tiled=True)  19.4 us
    all_gather x1, waiting for transfers between devices, per_device(): normed_all = lax.all_gather(normed, 'tp', axis=0, tiled=True)  19 us
    dot_general x1, matrix products, per_device(): jnp.dot(hidden, down_whole, preferred_element_type=jnp.float32)  16.5 us
  transfers between devices with their start and end apart: 6, of which 6 were waited for; matrix products, arithmetic and copies ran while one was open for 1% of the time, Pallas kernels for 0%

commit v1 on v0

--- a/solution.py
+++ b/solution.py
@@ -1,8 +1,17 @@
+import functools
 import math
 import jax
 import jax.numpy as jnp
 from jax import lax
 from jax.sharding import PartitionSpec as P
+
+
+def stocks_write(xs, join_dim):
+    z = lax.all_gather(xs, "sp")
+    return jnp.concatenate(z, axis=join_dim)
+
+
+convert_the_tiles = functools.partial(stocks_write, join_dim=1)
 
 
 def per_device(queries, keys, values, cum_gate, residual, w_out, gain, w_up, w_down):
@@ -67,7 +76,7 @@
         preferred_element_type=jnp.float32,
     )
     hidden = jnp.square(jax.nn.relu(up_proj)).astype(jnp.bfloat16)
-    down_whole = lax.all_gather(w_down, "sp", axis=1, tiled=True)
+    down_whole = convert_the_tiles(w_down)
     rounded = jnp.dot(hidden, down_whole, preferred_element_type=jnp.float32).astype(jnp.bfloat16)
     branch_out = lax.psum_scatter(
         lax.optimization_barrier(rounded).astype(jnp.float32).astype(jnp.bfloat16),

time: 502 us -> 441 us (0.88)
  waiting for transfers between devices: 368 us -> 293 us
  local copies, waits for them, and re-layouts: 18 us -> 29.8 us
    all_gather x1, waiting for transfers between devices: 125 us -> 59.6 us  [stocks_write(): z = lax.all_gather(xs, 'sp')]
    reshape x0 -> x1, local copies, waits for them, and re-layouts: none -> 11.6 us  [stocks_write(): return jnp.concatenate(z, axis=join_dim)]
    all_gather x1, waiting for transfers between devices: 19 us -> 10.6 us  [per_device(): normed_all = lax.all_gather(normed, 'tp', axis=0, tiled=True)]
  transfers between devices with their start and end apart: 6 -> 6, of which waited for: 6 -> 6; matrix products, arithmetic and copies ran while one was open for 1% -> 16% of each run, Pallas kernels for 0% -> 0%
where the time goes in v1:
time: 441 us; the launch traced here: 440 us
  waiting for transfers between devices  293 us (66%)
  matrix products  41.4 us (9%)
  blocking collectives  41.2 us (9%)
  local copies, waits for them, and re-layouts  29.8 us (7%)
  other arithmetic  16.4 us (4%)
  between operations  13.6 us (3%)
    all_gather x1, waiting for transfers between devices, per_device(): lax.all_gather(w_up, 'sp', axis=0, tiled=True)  126 us
    all_gather x1, waiting for transfers between devices, stocks_write(): z = lax.all_gather(xs, 'sp')  59.6 us
    all_gather x1, waiting for transfers between devices, per_device(): value_rows = lax.all_gather(values, 'sp', axis=0, tiled=True)  45.8 us
    all_gather x1, blocking collectives, per_device(): all_gates = lax.all_gather(cum_gate, 'sp', axis=0, tiled=True)  32.7 us
    reduce_scatter x1, waiting for transfers between devices, per_device(): lax.psum_scatter(lax.optimization_barrier(rounded).astype(jnp.float32).as...  29.5 us
    all_gather x1, waiting for transfers between devices, per_device(): key_rows = lax.all_gather(keys, 'sp', axis=0, tiled=True)  18.6 us
    dot_general x1, matrix products, per_device(): jnp.dot(hidden, down_whole, preferred_element_type=jnp.float32)  16.5 us
    dot_general x2, matrix products, absorb_block(): jnp.einsum('qhk,khd->qhd', weights.astype(jnp.bfloat16), value_blk, prefe...  12.6 us
  transfers between devices with their start and end apart: 6, of which 6 were waited for; matrix products, arithmetic and copies ran while one was open for 16% of the time, Pallas kernels for 0%

profile of v1, /device:TPU:0, one launch (start us, length us, event | category | flops | bytes accessed | tf_op | source)
XLA Modules:
  0.0 439.9 jit_solution(5681036742826392756)
XLA Ops:
  6.5 0.0 copy-start
  6.5 0.0 all-gather.7.cloned.1.call-start
  6.5 0.7 all-gather.7.cloned.1.call-update
  7.3 0.0 all-gather.9.cloned.1.call-start
  7.3 0.7 all-gather.9.cloned.1.call-update
  8.0 0.0 all-gather.15.cloned.1.call-start
  8.1 0.7 all-gather.15.cloned.1.call-update
  8.7 0.0 all-gather.11.cloned.1.call-start
  8.8 1.1 copy.17
  9.9 0.2 copy.19
  10.1 32.7 %all_gather.22 = f32[4096,2]{0,1:T(2,128)S(1)} all-gather(f32[512,2]{0,1:T(2,128)} %param.14), channel_id=1, replica_groups=mesh['sp'=8,'tp'=4] {'sp'}, dimensions={0}, use_global_device_ids=true | all-gather | bytes 36864 | tf_op jit(solution)/shard_map/all_gather | solution.py:25
  42.8 18.6 %all-gather.7.cloned.1.call-done = bf16[4096,256]{1,0:T(8,128)(2,1)} async-done(((bf16[512,256]{1,0:T(8,128)(2,1)}), bf16[4096,256]{1,0:T(8,128)(2,1)}) %all-gather.7.cloned.1.call-update) | async-done | bytes 2097168 | tf_op jit(solution)/shard_map/all_gather | solution.py:32
  61.4 4.0 reshape.68
  65.4 45.8 %all-gather.9.cloned.1.call-done = bf16[4096,256]{1,0:T(8,128)(2,1)} async-done(((bf16[512,256]{1,0:T(8,128)(2,1)}), bf16[4096,256]{1,0:T(8,128)(2,1)}) %all-gather.9.cloned.1.call-update) | async-done | bytes 2097168 | tf_op jit(solution)/shard_map/all_gather | solution.py:33
  111.2 4.0 reshape.70
  115.1 0.0 copy-done
  115.1 46.6 %while.15 = (s32[]{:T(128)}, f32[512,2]{0,1:T(2,128)S(1)}, f32[512,2]{0,1:T(2,128)S(1)}, f32[512,2,128]{0,2,1:T(8,128)}, s32[2]{0:T(128)S(1)}, /*index=5*/bf16[2...) while((s32[]{:T(128)}, f32[512,2]{0,1:T(2,128)S(1)}, ...), condition=%wide.region_3.4_spmd.clone, body=%wide.region_0.3_spmd.clone.sunk | while | flops 1110842880 | bytes 39239884 | solution.py:64
  115.1 0.6 dynamic_slice.26
  117.7 0.1 dynamic-slice_bitcast_fusion.2
  117.8 0.6 iota_add_fusion.5
  118.4 0.8 broadcast_compare_fusion.2
  119.2 2.8 constant_dynamic-slice_fusion.3
  122.0 4.5 %fusion.40 = (f32[512,2]{0,1:T(2,128)S(1)}, f32[2,2048,512]{2,1,0:T(8,128)}) fusion(f32[2,2048]{1,0:T(2,128)S(1)} %dynamic-slice_bitcast_fusion.2, f32[512,2]{0,1:T(2,128)S(1)} %get-tuple-element.270, pred[512,2048]{0,1:T(8,128)(4,1)S(1)} %broadcast_compare_fusion.2, bf16[512,2,128]{2,0,1:T(8,128)(2,1)S(1)} %get-tuple-element.269, ...), kind=kOutput, calls=%fused_computation.7.clone.1 | convolution fusion | flops 547355648 | bytes 10772480 | tf_op jit(solution)/shard_map/while/body/eval_jaxpr/qhd,khd->qhk/dot_general | solution.py:45
  126.6 4.8 %fusion.42 = f32[512,2]{0,1:T(2,128)S(1)} fusion(f32[2,2048,512]{2,1,0:T(8,128)} %get-tuple-element.231, f32[512,2]{0,1:T(2,128)S(1)} %fusion.41, f32[2,2048]{1,0:T(2,128)S(1)} %dynamic-slice_bitcast_fusion.2, f32[512,2]{0,1:T(2,128)S(1)} %get-tuple-element.270, pred[512,2048]{0,1:T(8,128)(4,1)S(1)} %broadcast_compare_fusion.2), kind=kLoop, calls=%fused_computation.6.clone.1 | loop fusion | flops 12581888 | bytes 9465856 | tf_op jit(solution)/shard_map/while/body/eval_jaxpr/reduce_sum | solution.py:54
  131.4 0.8 copy.35
  132.2 6.3 %fusion.44 = f32[512,2,128]{0,2,1:T(8,128)} fusion(f32[2,2048,512]{2,1,0:T(8,128)} %get-tuple-element.231, f32[512,2]{0,1:T(2,128)S(1)} %fusion.41, f32[2,2048]{1,0:T(2,128)S(1)} %dynamic-slice_bitcast_fusion.2, f32[512,2]{0,1:T(2,128)S(1)} %get-tuple-element.270, pred[512,2048]{0,1:T(8,128)(4,1)S(1)} %broadcast_compare_fusion.2, ...), kind=kOutput, calls=%fused_computation.12.clone.1 | convolution fusion | flops 549847040 | bytes 11563009 | tf_op jit(solution)/shard_map/while/body/eval_jaxpr/qhk,khd->qhd/dot_general | solution.py:55
  138.5 0.6 dynamic_slice.26
  141.0 0.1 dynamic-slice_bitcast_fusion.2
  141.1 0.6 iota_add_fusion.5
  141.7 0.8 broadcast_compare_fusion.2
  142.5 2.7 constant_dynamic-slice_fusion.3
  145.2 4.6 %fusion.40 = (f32[512,2]{0,1:T(2,128)S(1)}, f32[2,2048,512]{2,1,0:T(8,128)}) fusion(f32[2,2048]{1,0:T(2,128)S(1)} %dynamic-slice_bitcast_fusion.2, f32[512,2]{0,1:T(2,128)S(1)} %get-tuple-element.270, pred[512,2048]{0,1:T(8,128)(4,1)S(1)} %broadcast_compare_fusion.2, bf16[512,2,128]{2,0,1:T(8,128)(2,1)S(1)} %get-tuple-element.269, ...), kind=kOutput, calls=%fused_computation.7.clone.1 | convolution fusion | flops 547355648 | bytes 10772480 | tf_op jit(solution)/shard_map/while/body/eval_jaxpr/qhd,khd->qhk/dot_general | solution.py:45
  149.8 4.8 %fusion.42 = f32[512,2]{0,1:T(2,128)S(1)} fusion(f32[2,2048,512]{2,1,0:T(8,128)} %get-tuple-element.231, f32[512,2]{0,1:T(2,128)S(1)} %fusion.41, f32[2,2048]{1,0:T(2,128)S(1)} %dynamic-slice_bitcast_fusion.2, f32[512,2]{0,1:T(2,128)S(1)} %get-tuple-element.270, pred[512,2048]{0,1:T(8,128)(4,1)S(1)} %broadcast_compare_fusion.2), kind=kLoop, calls=%fused_computation.6.clone.1 | loop fusion | flops 12581888 | bytes 9465856 | tf_op jit(solution)/shard_map/while/body/eval_jaxpr/reduce_sum | solution.py:54
  154.6 0.8 copy.35
  155.4 6.4 %fusion.44 = f32[512,2,128]{0,2,1:T(8,128)} fusion(f32[2,2048,512]{2,1,0:T(8,128)} %get-tuple-element.231, f32[512,2]{0,1:T(2,128)S(1)} %fusion.41, f32[2,2048]{1,0:T(2,128)S(1)} %dynamic-slice_bitcast_fusion.2, f32[512,2]{0,1:T(2,128)S(1)} %get-tuple-element.270, pred[512,2048]{0,1:T(8,128)(4,1)S(1)} %broadcast_compare_fusion.2, ...), kind=kOutput, calls=%fused_computation.12.clone.1 | convolution fusion | flops 549847040 | bytes 11563009 | tf_op jit(solution)/shard_map/while/body/eval_jaxpr/qhk,khd->qhd/dot_general | solution.py:55
  161.8 0.0 copy-start.1
  161.8 1.1 divide_convert_fusion
  162.9 0.1 reshape.74
  162.9 0.2 copy.25
  163.1 8.5 %all_to_all.16 = bf16[4,128,256]{2,1,0:T(8,128)(2,1)S(1)} all-to-all(bf16[4,128,256]{2,1,0:T(8,128)(2,1)S(1)} %copy.25), channel_id=1, replica_groups=mesh['sp'=8,'tp'=4] {'tp'}, dimensions={0} | all-to-all | bytes 524288 | tf_op jit(solution)/shard_map/all_to_all | solution.py:67
  171.6 0.2 copy.22
  171.8 3.2 multiply_reduce_fusion
  175.0 0.0 copy-done.1
  175.0 0.9 multiply_convert_fusion.1
  175.9 0.0 all-gather.11.cloned.1.call-update
  176.0 0.0 all-gather.13.cloned.1.call-start
  176.0 0.5 all-gather.13.cloned.1.call-update
  176.6 0.2 reduce-scatter.2.cloned.1.call-start
  176.8 59.6 %all-gather.15.cloned.1.call-done = bf16[16384,256]{1,0:T(8,128)(2,1)} async-done(((bf16[2048,256]{1,0:T(8,128)(2,1)}), bf16[16384,256]{1,0:T(8,128)(2,1)}) %all-gather.15.cloned.1.call-update) | async-done | bytes 8388624 | tf_op jit(solution)/shard_map/all_gather | solution.py:10
  236.4 11.6 %copy.23 = bf16[2048,8,256]{0,2,1:T(8,128)(2,1)} copy(bf16[2048,8,256]{2,0,1:T(8,128)(2,1)} %bitcast.65) | data formatting | bytes 16777216 | tf_op jit(solution)/shard_map/reshape | solution.py:11
  248.0 10.6 %all-gather.11.cloned.1.call-done = bf16[512,2048]{1,0:T(8,128)(2,1)} async-done(((bf16[128,2048]{1,0:T(8,128)(2,1)}), bf16[512,2048]{1,0:T(8,128)(2,1)}) %all-gather.11.cloned.1.call-update) | async-done | bytes 2097168 | tf_op jit(solution)/shard_map/all_gather | solution.py:72
  258.6 126.5 %all-gather.13.cloned.1.call-done = bf16[2048,2048]{1,0:T(8,128)(2,1)} async-done(((bf16[256,2048]{1,0:T(8,128)(2,1)}), bf16[2048,2048]{1,0:T(8,128)(2,1)}) %all-gather.13.cloned.1.call-update) | async-done | bytes 8388624 | tf_op jit(solution)/shard_map/all_gather | solution.py:75
  385.1 16.5 %convolution_convert_fusion = bf16[512,2048]{1,0:T(8,128)(2,1)} fusion(bf16[2048,2048]{0,1:T(8,128)(2,1)} %bitcast.66, bf16[512,2048]{1,0:T(8,128)(2,1)} %all-gather.11.cloned.1.call-done, bf16[2048,2048]{1,0:T(8,128)(2,1)} %all-gather.13.cloned.1.call-done), kind=kOutput, calls=%fused_computation.30 | convolution fusion | flops 8594128896 | bytes 20971520 | tf_op jit(solution)/shard_map/dot_general | solution.py:80
  401.6 0.0 reduce-scatter.2.cloned.1.call-update
  401.6 29.5 %reduce-scatter.2.cloned.1.call-done = bf16[128,2048]{1,0:T(8,128)(2,1)} async-done(((bf16[512,2048]{1,0:T(8,128)(2,1)}), bf16[128,2048]{1,0:T(8,128)(2,1)}) %reduce-scatter.2.cloned.1.call-update) | async-done | bytes 524304 | tf_op jit(solution)/shard_map/reduce_scatter | solution.py:81
  431.1 1.9 add_convert_fusion
  (13 shorter events, 0.1 us)
Async XLA Ops:
  6.5 108.6 %copy-start = (f32[512,2]{0,1:T(2,128)S(1)}, f32[512,2]{0,1:T(2,128)}, u32[]{:S(2)}) copy-start(f32[512,2]{0,1:T(2,128)} %param.14) | copy-start | bytes 12292
  6.5 54.9 %all-gather.7.cloned.1.call-start = ((), (), s32[]{:S(2)}) async-start(), calls=%async_computation.2 | async-start | bytes 2359296 | tf_op jit(solution)/shard_map/all_gather | solution.py:32
  7.3 103.9 %all-gather.9.cloned.1.call-start = ((), (), s32[]{:S(2)}) async-start(), calls=%async_computation.3 | async-start | bytes 2359296 | tf_op jit(solution)/shard_map/all_gather | solution.py:33
  8.0 228.4 %all-gather.15.cloned.1.call-start = ((), (), s32[]{:S(2)}) async-start(), calls=%async_computation.7 | async-start | bytes 9437184 | tf_op jit(solution)/shard_map/all_gather | solution.py:10
  8.7 249.8 %all-gather.11.cloned.1.call-start = ((), (), s32[]{:S(2)}) async-start(), calls=%async_computation.4 | async-start | bytes 2621440 | tf_op jit(solution)/shard_map/all_gather | solution.py:72
  161.8 13.2 %copy-start.1 = (f32[2048]{0:T(1024)S(1)}, f32[2048]{0:T(1024)}, u32[]{:S(2)}) copy-start(f32[2048]{0:T(1024)} %param.17) | copy-start | bytes 24580
  176.0 209.1 %all-gather.13.cloned.1.call-start = ((), (), s32[]{:S(2)}) async-start(), calls=%async_computation.5 | async-start | bytes 9437184 | tf_op jit(solution)/shard_map/all_gather | solution.py:75
  176.6 254.5 %reduce-scatter.2.cloned.1.call-start = ((), (), s32[]{:S(2)}) async-start(), calls=%async_computation.6 | async-start | bytes 2621440 | tf_op jit(solution)/shard_map/reduce_scatter | solution.py:81
Sparse Core Ops, SparseCore 0:
  9.5 51.8 all-gather.6
  63.5 47.6 all-gather.8
  113.3 123.0 all-gather.14
  237.8 20.7 all-gather.10
  260.6 124.4 all-gather.12
  401.7 29.3 reduce-scatter.1
